TPU v7x, 32 devices: a whole 2x2x4 slice. The times are simulated.
32 devices in a mesh: grp: 2 (over y), fs: 4 (over z), tp: 4 (over x, core).
Axes of the slice: x: 2, y: 2, z: 4, core: 2. Of those that a mesh axis runs over, the one named last changes fastest.
Arguments:
- tokens: bfloat16 [1536, 2048], P(('grp', 'fs'), 'tp'), parts along dimension 0, may hold values from -40 to 40
- routes: int32 [1536, 2], P(('grp', 'fs')), parts along dimension 0, may hold values from 0 to 3, all different within a row; in each aligned block of 192 rows (0 to 191, 192 to 383, ...) at most 112 rows name the same one
- routing_weight: float32 [1536, 2], P(('grp', 'fs')), parts along dimension 0, may hold values from 0.1 to 0.6
- norm_gain_vector: float32 [2048], P('tp'), may hold values from 0.1 to 1.9
- expert_gate: float32 [4, 512, 2048], P(None, 'fs', 'tp'), may hold values from -0.125 to 0.125
- expert_up: float32 [4, 512, 2048], P(None, 'fs', 'tp'), may hold values from -0.125 to 0.125
- expert_down: float32 [4, 512, 2048], P(None, 'fs', 'tp'), may hold values from -0.25 to 0.25
- shared_gate: float32 [512, 2048], P('fs', 'tp'), may hold values from -0.125 to 0.125
- shared_up: float32 [512, 2048], P('fs', 'tp'), may hold values from -0.125 to 0.125
- shared_down: float32 [512, 2048], P('fs', 'tp'), may hold values from -0.25 to 0.25
Outputs:
- mixed: bfloat16 [1536, 2048], P(('grp', 'fs'), 'tp'), parts along dimension 0
- gate_served: bfloat16 [8, 512, 2048], P(('grp', 'fs'), None, 'tp'), parts along dimension 0
- up_served: bfloat16 [8, 512, 2048], P(('grp', 'fs'), None, 'tp'), parts along dimension 0
- down_served: bfloat16 [8, 512, 2048], P(('grp', 'fs'), None, 'tp'), parts along dimension 0
- shared_gate_served: bfloat16 [1024, 2048], P('grp', 'tp'), parts along dimension 0
- shared_up_served: bfloat16 [1024, 2048], P('grp', 'tp'), parts along dimension 0
- shared_down_served: bfloat16 [1024, 2048], P('grp', 'tp'), parts along dimension 0
There are 2 independent parts, one for each index of `grp`. A program takes and returns all parts, laid end to end along the dimension named above; an argument that names none is the same for every part. Nothing has to cross between parts.
Inputs may be any that keep to these rules, and one draw needn't show every extreme that they name: `routes`: each row names 2 different experts. In each aligned block of 192 rows no expert is named by more than 112 rows, and in some block an expert is named by exactly 112 rows.
All inputs are finite; a program needn't handle non-finite values.
Results may differ from a plain program's by a relative error of at most 0.022.
Values may be sent and summed in bfloat16 or wider, within the bound.
A program may use at most 64 MiB of HBM per device.

v0:
```python
import jax
import jax.numpy as jnp
from jax import lax
from jax.sharding import PartitionSpec as P

norm_eps = 1e-06


def dense_rows(rows, weight):
    return lax.dot_general(
        rows, weight, (((1,), (1,)), ((), ())), preferred_element_type=jnp.float32
    )


def per_device(
    tokens,
    routes,
    routing_weight,
    norm_gain_vector,
    expert_gate,
    expert_up,
    expert_down,
    shared_gate,
    shared_up,
    shared_down,
):
    tok_rows, portion_width = tokens.shape
    model_width = portion_width * lax.axis_size("tp")
    experts = expert_gate.shape[0]
    top_count = routes.shape[1]
    capacity = tok_rows * top_count * 7 // (6 * experts)
    gate_round = (expert_gate * norm_gain_vector[None, None, :]).astype(jnp.bfloat16)
    up_round = (expert_up * norm_gain_vector[None, None, :]).astype(jnp.bfloat16)
    down_round = expert_down.astype(jnp.bfloat16)
    gate_refreshed, up_new, down_new = (
        lax.all_to_all(gate_round, "fs", split_axis=0, concat_axis=1, tiled=True),
        lax.all_to_all(up_round, "fs", split_axis=0, concat_axis=1, tiled=True),
        lax.all_to_all(down_round, "fs", split_axis=0, concat_axis=1, tiled=True),
    )
    shared_g, shared_u, shared_d = (
        lax.all_gather(
            (shared_gate * norm_gain_vector[None, :]).astype(jnp.bfloat16), "fs", axis=0, tiled=True
        ),
        lax.all_gather(
            (shared_up * norm_gain_vector[None, :]).astype(jnp.bfloat16), "fs", axis=0, tiled=True
        ),
        lax.all_gather(shared_down.astype(jnp.bfloat16), "fs", axis=0, tiled=True),
    )
    values = tokens.astype(jnp.float32)
    totals = lax.psum(jnp.sum(values * values, axis=1), "tp")
    normed = (values * lax.rsqrt(totals / model_width + norm_eps)[:, None]).astype(jnp.bfloat16)
    flat_expert = routes.reshape(-1)
    onehot = (flat_expert[:, None] == jnp.arange(experts, dtype=jnp.int32)[None, :]).astype(
        jnp.int32
    )
    earlier = jnp.cumsum(onehot, axis=0) - onehot
    slot_index = jnp.sum(earlier * onehot, axis=1)
    target = (flat_expert * capacity + slot_index).reshape(tok_rows, top_count)
    places = jnp.arange(experts * capacity, dtype=jnp.int32)
    placing = jnp.sum(
        (target[:, :, None] == places[None, None, :]).astype(jnp.int32), axis=1
    ).astype(jnp.bfloat16)
    outgoing = lax.dot_general(
        placing, normed, (((0,), (0,)), ((), ())), preferred_element_type=jnp.float32
    ).astype(jnp.bfloat16)
    incoming = lax.all_to_all(
        outgoing.reshape(experts, capacity, portion_width),
        "fs",
        split_axis=0,
        concat_axis=0,
        tiled=True,
    )
    arrived = incoming.reshape(experts * capacity, portion_width)
    partials = (
        dense_rows(arrived, gate_refreshed[0]).astype(jnp.bfloat16),
        dense_rows(arrived, up_new[0]).astype(jnp.bfloat16),
        dense_rows(normed, shared_g).astype(jnp.bfloat16),
        dense_rows(normed, shared_u).astype(jnp.bfloat16),
    )
    gate_part, up_part, sgate_part, sup_part = (
        lax.psum_scatter(partials[0], "tp", scatter_dimension=1, tiled=True).astype(jnp.float32),
        lax.psum_scatter(partials[1], "tp", scatter_dimension=1, tiled=True).astype(jnp.float32),
        lax.psum_scatter(partials[2], "tp", scatter_dimension=1, tiled=True).astype(jnp.float32),
        lax.psum_scatter(partials[3], "tp", scatter_dimension=1, tiled=True).astype(jnp.float32),
    )
    hidden, shared_hidden = (
        lax.all_gather(
            (jax.nn.silu(gate_part) * up_part).astype(jnp.bfloat16), "tp", axis=1, tiled=True
        ),
        lax.all_gather(
            (jax.nn.silu(sgate_part) * sup_part).astype(jnp.bfloat16), "tp", axis=1, tiled=True
        ),
    )
    produced = jnp.dot(hidden, down_new[0], preferred_element_type=jnp.float32).astype(jnp.bfloat16)
    returned = lax.all_to_all(
        produced.reshape(experts, capacity, portion_width),
        "fs",
        split_axis=0,
        concat_axis=0,
        tiled=True,
    )
    picked = returned.reshape(experts * capacity, portion_width)[target]
    routed = jnp.sum(routing_weight[:, :, None] * picked.astype(jnp.float32), axis=1)
    shared_out = jnp.dot(shared_hidden, shared_d, preferred_element_type=jnp.float32)
    mixed = (routed + shared_out).astype(jnp.bfloat16)
    return (mixed, gate_refreshed, up_new, down_new, shared_g, shared_u, shared_d)


def solution(mesh):
    return jax.shard_map(
        per_device,
        mesh=mesh,
        in_specs=(
            P(("grp", "fs"), "tp"),
            P(("grp", "fs"), None),
            P(("grp", "fs"), None),
            P("tp"),
            P(None, "fs", "tp"),
            P(None, "fs", "tp"),
            P(None, "fs", "tp"),
            P("fs", "tp"),
            P("fs", "tp"),
            P("fs", "tp"),
        ),
        out_specs=(
            P(("grp", "fs"), "tp"),
            P(("grp", "fs"), None, "tp"),
            P(("grp", "fs"), None, "tp"),
            P(("grp", "fs"), None, "tp"),
            P("grp", "tp"),
            P("grp", "tp"),
            P("grp", "tp"),
        ),
        check_vma=False,
    )
```

profile of v0, /device:TPU:0, one launch (start us, length us, event | category | flops | bytes accessed | tf_op | source)
XLA Modules:
  0.0 186.0 jit_solution(6550005453519456522)
XLA Ops:
  8.3 1.2 reduce-window.6
  11.9 8.5 %psum.7 = f32[192]{0:T(256)S(1)} all-reduce(f32[192]{0:T(256)S(1)} %fusion.1), channel_id=1, replica_groups=mesh['grp'=2,'fs'=4,'tp'=4] {'tp'}, use_global_device_ids=true, to_apply=%region_5.6 | all-reduce | flops 192 | bytes 1536 | tf_op jit(solution)/shard_map/psum | solution.py:50
  20.4 1.1 convolution_convert_fusion.3
  21.5 5.0 %all-to-all-start = ((bf16[4,112,512]{2,1,0:T(8,128)(2,1)}), bf16[4,112,512]{2,1,0:T(8,128)(2,1)S(1)}, u32[]{:S(2)}, u32[]{:S(2)}) async-start(bf16[4,112,512]{2,1,0:T(8,128)(2,1)} %bitcast.1), calls=%async_computation | async-start | bytes 917504 | tf_op jit(solution)/shard_map/all_to_all | solution.py:66
  26.5 2.3 %multiply_convert_fusion.1 = (bf16[4,128,512]{2,1,0:T(8,128)(2,1)S(1)}, bf16[4,128,512]{2,1,0:T(8,128)(2,1)}) fusion(f32[4,128,512]{2,1,0:T(8,128)S(1)} %copy-done.3, f32[512]{0:T(512)S(1)} %copy-done.9, f32[4,128,512]{2,1,0:T(8,128)} %param.15), kind=kLoop, calls=%fused_computation.10 | loop fusion | flops 1048576 | bytes 3147776 | tf_op jit(solution)/shard_map/convert_element_type | solution.py:32
  28.8 9.6 %all-to-all-done = bf16[4,112,512]{2,1,0:T(8,128)(2,1)S(1)} async-done(((bf16[4,112,512]{2,1,0:T(8,128)(2,1)}), bf16[4,112,512]{2,1,0:T(8,128)(2,1)S(1)}, u32[]{:S(2)}, u32[]{:S(2)}) %all-to-all-start) | async-done | bytes 458784 | tf_op jit(solution)/shard_map/all_to_all | solution.py:66
  38.4 15.7 %all_to_all.46 = bf16[4,128,512]{2,1,0:T(8,128)(2,1)S(1)} all-to-all(bf16[4,128,512]{2,1,0:T(8,128)(2,1)S(1)} %get-tuple-element.11), channel_id=1, replica_groups=mesh['grp'=2,'fs'=4,'tp'=4] {'fs'}, dimensions={0} | all-to-all | bytes 1048576 | tf_op jit(solution)/shard_map/all_to_all | solution.py:36
  54.1 3.5 %all-to-all-start.2 = ((bf16[4,128,512]{2,1,0:T(8,128)(2,1)}), bf16[4,128,512]{2,1,0:T(8,128)(2,1)S(1)}, u32[]{:S(2)}, u32[]{:S(2)}) async-start(bf16[4,128,512]{2,1,0:T(8,128)(2,1)} %get-tuple-element.12), calls=%async_computation.2 | async-start | bytes 1048576 | tf_op jit(solution)/shard_map/all_to_all | solution.py:37
  58.1 1.0 copy.40
  59.2 11.8 %all-to-all-done.2 = bf16[4,128,512]{2,1,0:T(8,128)(2,1)S(1)} async-done(((bf16[4,128,512]{2,1,0:T(8,128)(2,1)}), bf16[4,128,512]{2,1,0:T(8,128)(2,1)S(1)}, u32[]{:S(2)}, u32[]{:S(2)}) %all-to-all-start.2) | async-done | bytes 524320 | tf_op jit(solution)/shard_map/all_to_all | solution.py:37
  72.5 2.1 %convert_element_type.93 = bf16[4,128,512]{2,1,0:T(8,128)(2,1)} convert(f32[4,128,512]{2,1,0:T(8,128)} %param.16) | non-fusion elementwise | flops 262144 | bytes 1572864 | tf_op jit(solution)/shard_map/convert_element_type | solution.py:34
  74.6 3.6 %all-to-all-start.3 = ((bf16[4,128,512]{2,1,0:T(8,128)(2,1)}), bf16[4,128,512]{2,1,0:T(8,128)(2,1)S(1)}, u32[]{:S(2)}, u32[]{:S(2)}) async-start(bf16[4,128,512]{2,1,0:T(8,128)(2,1)} %convert_element_type.93), calls=%async_computation.3 | async-start | bytes 1048576 | tf_op jit(solution)/shard_map/all_to_all | solution.py:38
  78.3 24.3 %all_gather.16 = bf16[512,512]{1,0:T(8,128)(2,1)S(1)} all-gather(bf16[128,512]{1,0:T(8,128)(2,1)S(1)} %get-tuple-element.9), channel_id=1, replica_groups=mesh['grp'=2,'fs'=4,'tp'=4] {'fs'}, dimensions={0}, use_global_device_ids=true | all-gather | bytes 655360 | tf_op jit(solution)/shard_map/all_gather | solution.py:41
  103.8 15.2 %all_gather.17 = bf16[512,512]{1,0:T(8,128)(2,1)S(1)} all-gather(bf16[128,512]{1,0:T(8,128)(2,1)S(1)} %get-tuple-element.10), channel_id=1, replica_groups=mesh['grp'=2,'fs'=4,'tp'=4] {'fs'}, dimensions={0}, use_global_device_ids=true | all-gather | bytes 655360 | tf_op jit(solution)/shard_map/all_gather | solution.py:44
  120.3 1.0 copy.41
  121.3 1.0 copy.43
  122.5 7.6 %all_gather.15 = bf16[448,512]{1,0:T(8,128)(2,1)S(1)} all-gather(bf16[448,128]{1,0:T(8,128)(2,1)S(1)} %fusion.7), channel_id=1, replica_groups=mesh['grp'=2,'fs'=4,'tp'=4] {'tp'}, dimensions={1}, use_global_device_ids=true | all-gather | bytes 573440 | tf_op jit(solution)/shard_map/all_gather | solution.py:87
  130.0 1.2 convolution_convert_fusion
  131.2 5.4 %all-to-all-start.4 = ((bf16[4,112,512]{2,1,0:T(8,128)(2,1)}), bf16[4,112,512]{2,1,0:T(8,128)(2,1)S(1)}, u32[]{:S(2)}, u32[]{:S(2)}) async-start(bf16[4,112,512]{2,1,0:T(8,128)(2,1)} %bitcast.6), calls=%async_computation.4 | async-start | bytes 917504 | tf_op jit(solution)/shard_map/all_to_all | solution.py:95
  137.5 22.6 %all_gather.19 = bf16[512,512]{1,0:T(8,128)(2,1)S(1)} all-gather(bf16[128,512]{1,0:T(8,128)(2,1)S(1)} %convert_element_type.103), channel_id=1, replica_groups=mesh['grp'=2,'fs'=4,'tp'=4] {'fs'}, dimensions={0}, use_global_device_ids=true | all-gather | bytes 655360 | tf_op jit(solution)/shard_map/all_gather | solution.py:47
  162.1 6.1 %all_gather.18 = bf16[192,512]{1,0:T(8,128)(2,1)} all-gather(bf16[192,128]{1,0:T(8,128)(2,1)S(1)} %fusion.13), channel_id=1, replica_groups=mesh['grp'=2,'fs'=4,'tp'=4] {'tp'}, dimensions={1}, use_global_device_ids=true | all-gather | bytes 245760 | tf_op jit(solution)/shard_map/all_gather | solution.py:90
  168.2 2.6 %gather_fusion = bf16[384,512]{1,0:T(8,128)(2,1)} fusion(bf16[448,512]{1,0:T(8,128)(2,1)S(1)} %bitcast.47, s32[1024]{0:T(1024)S(1)} %pad_clamp_fusion), kind=kCustom, calls=%fused_computation | custom fusion | bytes 787968 | tf_op jit(solution)/shard_map/gather | solution.py:102
  170.8 1.5 reshape.86
  172.3 1.0 multiply_reduce_fusion
  (74 shorter events, 17.2 us)
Async XLA Ops:
  10.1 0.7 copy-start.8
  10.8 0.9 copy-start.2
  11.8 14.8 %copy-start.3 = (f32[4,128,512]{2,1,0:T(8,128)S(1)}, f32[4,128,512]{2,1,0:T(8,128)}, u32[]{:S(2)}) copy-start(f32[4,128,512]{2,1,0:T(8,128)} %param.14) | copy-start | bytes 3145732
  21.5 5.0 %copy-start.9 = (f32[512]{0:T(512)S(1)}, f32[512]{0:T(512)}, u32[]{:S(2)}) copy-start(f32[512]{0:T(512)} %param.13) | copy-start | bytes 6148
  21.5 16.9 %all-to-all-start = ((bf16[4,112,512]{2,1,0:T(8,128)(2,1)}), bf16[4,112,512]{2,1,0:T(8,128)(2,1)S(1)}, u32[]{:S(2)}, u32[]{:S(2)}) async-start(bf16[4,112,512]{2,1,0:T(8,128)(2,1)} %bitcast.1), calls=%async_computation | async-start | bytes 917504 | tf_op jit(solution)/shard_map/all_to_all | solution.py:66
  54.1 16.9 %all-to-all-start.2 = ((bf16[4,128,512]{2,1,0:T(8,128)(2,1)}), bf16[4,128,512]{2,1,0:T(8,128)(2,1)S(1)}, u32[]{:S(2)}, u32[]{:S(2)}) async-start(bf16[4,128,512]{2,1,0:T(8,128)(2,1)} %get-tuple-element.12), calls=%async_computation.2 | async-start | bytes 1048576 | tf_op jit(solution)/shard_map/all_to_all | solution.py:37
  57.6 62.6 %reduce-scatter.13.cloned.1.call-start = ((), (), s32[]{:S(2)}) async-start(), calls=%async_computation.9 | async-start | bytes 655360
  59.1 62.2 %reduce-scatter.15.cloned.1.call-start = ((), (), s32[]{:S(2)}) async-start(), calls=%async_computation.10 | async-start | bytes 655360
  74.6 3.7 %copy-start.5 = (f32[128,512]{1,0:T(8,128)S(1)}, f32[128,512]{1,0:T(8,128)}, u32[]{:S(2)}) copy-start(f32[128,512]{1,0:T(8,128)} %param.17) | copy-start | bytes 786436
  74.6 3.7 %copy-start.6 = (f32[128,512]{1,0:T(8,128)S(1)}, f32[128,512]{1,0:T(8,128)}, u32[]{:S(2)}) copy-start(f32[128,512]{1,0:T(8,128)} %param.18) | copy-start | bytes 786436
  74.6 55.4 %all-to-all-start.3 = ((bf16[4,128,512]{2,1,0:T(8,128)(2,1)}), bf16[4,128,512]{2,1,0:T(8,128)(2,1)S(1)}, u32[]{:S(2)}, u32[]{:S(2)}) async-start(bf16[4,128,512]{2,1,0:T(8,128)(2,1)} %convert_element_type.93), calls=%async_computation.3 | async-start | bytes 1048576 | tf_op jit(solution)/shard_map/all_to_all | solution.py:38
  78.2 81.9 %reduce-scatter.17.cloned.1.call-start = ((), (), s32[]{:S(2)}) async-start(), calls=%async_computation.11 | async-start | bytes 327680
  103.8 57.3 %reduce-scatter.19.cloned.1.call-start = ((), (), s32[]{:S(2)}) async-start(), calls=%async_computation.12 | async-start | bytes 327680
  130.0 1.2 copy-start
  131.2 5.6 %copy-start.10 = (f32[192,2]{0,1:T(2,128)S(1)}, f32[192,2]{0,1:T(2,128)}, u32[]{:S(2)}) copy-start(f32[192,2]{0,1:T(2,128)} %param.12) | copy-start | bytes 4612
  131.2 37.0 %all-to-all-start.4 = ((bf16[4,112,512]{2,1,0:T(8,128)(2,1)}), bf16[4,112,512]{2,1,0:T(8,128)(2,1)S(1)}, u32[]{:S(2)}, u32[]{:S(2)}) async-start(bf16[4,112,512]{2,1,0:T(8,128)(2,1)} %bitcast.6), calls=%async_computation.4 | async-start | bytes 917504 | tf_op jit(solution)/shard_map/all_to_all | solution.py:95
  136.6 0.9 copy-start.7
  172.3 1.0 copy-start.4
  175.1 1.2 copy-start.1
Sparse Core Ops, SparseCore 0:
  61.5 23.8 reduce-scatter.12
  88.4 21.6 reduce-scatter.14
  113.2 20.0 reduce-scatter.16
  136.1 19.9 reduce-scatter.18
where the time goes:
time: 187 us; the launch traced here: 186 us
  blocking collectives  99.9 us (53%)
  waiting for transfers between devices  21.6 us (12%)
  local copies, waits for them, and re-layouts  20.8 us (11%)
  starting transfers between devices  17.6 us (9%)
  between operations  14 us (7%)
  other arithmetic  7.37 us (4%)
  matrix products  4.78 us (3%)
    all_gather x1, blocking collectives, per_device(): lax.all_gather((shared_gate * norm_gain_vector[None, :]).astype(jnp.bfloa...  24.3 us
    all_gather x1, blocking collectives, per_device(): lax.all_gather(shared_down.astype(jnp.bfloat16), 'fs', axis=0, tiled=True)  22.6 us
    unnamed x38, local copies, waits for them, and re-layouts  15.7 us
    all_to_all x1, blocking collectives, per_device(): lax.all_to_all(gate_round, 'fs', split_axis=0, concat_axis=1, tiled=True)  15.7 us
    all_gather x1, blocking collectives, per_device(): lax.all_gather((shared_up * norm_gain_vector[None, :]).astype(jnp.bfloat1...  15.2 us
    all_to_all x1, waiting for transfers between devices, per_device(): lax.all_to_all(up_round, 'fs', split_axis=0, concat_axis=1, tiled=True)  11.8 us
    all_to_all x1, waiting for transfers between devices, per_device(): lax.all_to_all(outgoing.reshape(experts, capacity, portion_width), 'fs',...  9.59 us
    psum x1, blocking collectives, per_device(): totals = lax.psum(jnp.sum(values * values, axis=1), 'tp')  8.5 us
  transfers between devices with their start and end apart: 8, of which 2 were waited for; matrix products, arithmetic and copies ran while one was open for 8% of the time, Pallas kernels for 0%

commit v1 on v0

--- a/solution.py
+++ b/solution.py
@@ -1,6 +1,10 @@
+import functools
+
 import jax
 import jax.numpy as jnp
 from jax import lax
+from jax.experimental import pallas as pl
+from jax.experimental.pallas import tpu as pltpu
 from jax.sharding import PartitionSpec as P
 
 norm_eps = 1e-06
@@ -12,7 +16,7 @@
     )
 
 
-def per_device(
+def per_device_plain(
     tokens,
     routes,
     routing_weight,
@@ -106,6 +110,353 @@
     return (mixed, gate_refreshed, up_new, down_new, shared_g, shared_u, shared_d)
 
 
+MESH = pl.DeviceIdType.MESH
+
+
+def nearest_first(n):
+    orders = [sorted(range(n), key=lambda s: (abs(s - f), s)) for f in range(n)]
+    return [sum(orders[f][i] * n**f for f in range(n)) for i in range(n)]
+
+
+def fused_kernel(
+    n_fs, n_tp, top_count,
+    tok_ref, meta_ref, gain_ref, eg_ref, eu_ref, ed_ref, sg_ref, su_ref, sd_ref,
+    mixed_ref, wout_ref,
+    wall, tokbuf, metabuf, ssown, ssbuf, scown, scbuf, mt, sct, part, rsbuf, hid, outf, outb, retbuf,
+    tok_s, tok_r, meta_s, meta_r, ss_s, ss_r, sc_s, sc_r, rs_s, rs_r, ag_s, ag_r,
+    ret_s, ret_r, we_s, we_r, ws_s, ws_r, ye_s, ye_r, ys_s, ys_r,
+):
+    g, f, t = lax.axis_index("grp"), lax.axis_index("fs"), lax.axis_index("tp")
+    rows, width = tok_ref.shape
+    experts, units = eg_ref.shape[0], eg_ref.shape[1]
+    sub = rows // n_tp
+    half = units // 2
+    f32, bf16 = jnp.float32, jnp.bfloat16
+    code = nearest_first(n_fs)
+
+    def source(i):
+        total = 0
+        digits = code[i]
+        picks = [(digits // n_fs**q) % n_fs for q in range(n_fs)]
+        for q in range(n_fs):
+            hit = 1 - jnp.minimum(1, jnp.abs(f - q))
+            total = total + picks[q] * hit
+        return total
+
+    def at_fs(index):
+        return (g, index, t)
+
+    def at_tp(index):
+        return (g, f, index)
+
+    partner = (1 - g, f, t)
+
+    def remote(src, dst, send, recv, device):
+        return pltpu.make_async_remote_copy(
+            src_ref=src, dst_ref=dst, send_sem=send, recv_sem=recv,
+            device_id=device, device_id_type=MESH,
+        )
+
+    fs_others = [lax.rem(f + j, n_fs) for j in range(1, n_fs)]
+    tp_others = [lax.rem(t + j, n_tp) for j in range(1, n_tp)]
+
+    barrier = pltpu.get_barrier_semaphore()
+    peers = [at_fs(d) for d in fs_others] + [at_tp(d) for d in tp_others] + [partner]
+    for device in peers:
+        pl.semaphore_signal(barrier, inc=1, device_id=device, device_id_type=MESH)
+    pl.semaphore_wait(barrier, len(peers))
+
+    def to_right(src, dst, send, recv):
+        @pl.when(f < n_fs - 1)
+        def _():
+            remote(src, dst, send, recv, at_fs(f + 1)).start()
+
+    def to_left(src, dst, send, recv):
+        @pl.when(f > 0)
+        def _():
+            remote(src, dst, send, recv, at_fs(f - 1)).start()
+
+    def onward(s, ref, send, recv):
+        @pl.when((s < f) & (f < n_fs - 1))
+        def _():
+            remote(ref, ref, send.at[s, 0], recv.at[s], at_fs(f + 1)).start()
+
+        @pl.when((s > f) & (f > 0))
+        def _():
+            remote(ref, ref, send.at[s, 1], recv.at[s], at_fs(f - 1)).start()
+
+    def line_sends_done(refs, send, recv):
+        for s in range(n_fs):
+            ref = refs(s)
+
+            @pl.when((f >= s) & (f < n_fs - 1))
+            def _():
+                remote(ref, ref, send.at[s, 0], recv.at[s], at_fs(f + 1)).wait_send()
+
+            @pl.when((f <= s) & (f > 0))
+            def _():
+                remote(ref, ref, send.at[s, 1], recv.at[s], at_fs(f - 1)).wait_send()
+
+    for go, way in ((to_right, 0), (to_left, 1)):
+        go(meta_ref, metabuf.at[f], meta_s.at[f, way], meta_r.at[f])
+        go(tok_ref, tokbuf.at[f], tok_s.at[f, way], tok_r.at[f])
+
+    x = tok_ref[...].astype(f32)
+    sq = x * x
+    high = sq.astype(bf16)
+    low = (sq - high.astype(f32)).astype(bf16)
+    ones = jnp.ones((8, width), bf16)
+    ssown[...] = jnp.zeros(ssown.shape, f32)
+    ssown[:, 0:rows] = dense_rows(ones, high) + dense_rows(ones, low)
+    for d in tp_others:
+        remote(ssown, ssbuf.at[t], ss_s.at[d], ss_r.at[t], at_tp(d)).start()
+
+    gain = gain_ref[...]
+    for e in range(experts):
+        wall[0, e] = (eg_ref[e] * gain).astype(bf16)
+        wall[1, e] = (eu_ref[e] * gain).astype(bf16)
+    wall[0, experts] = (sg_ref[...] * gain).astype(bf16)
+    wall[1, experts] = (su_ref[...] * gain).astype(bf16)
+
+    def transposed(row_ref):
+        return jnp.transpose(row_ref[...])[0:rows]
+
+    def forward_block(i, tokens, meta):
+        mt[i] = transposed(meta)
+        names = [mt[i, :, k : k + 1] for k in range(top_count)]
+        columns = []
+        for m in range(2):
+            weight = wall[m].reshape((experts + 1) * units, width)
+            sums = dense_rows(tokens[...], weight)
+            for name in names:
+                chosen = jnp.zeros((rows, units), f32)
+                for e in range(experts):
+                    chosen = jnp.where(name == float(e), sums[:, e * units : (e + 1) * units], chosen)
+                columns.append(chosen)
+            columns.append(sums[:, experts * units :])
+        for c, column in enumerate(columns):
+            part[i, :, :, c * units : (c + 1) * units] = column.astype(bf16).reshape(n_tp, sub, units)
+        for d in tp_others:
+            remote(part.at[i, d], rsbuf.at[i, t], rs_s.at[i, d], rs_r.at[i, t], at_tp(d)).start()
+
+    def hidden_block(i, scale_row):
+        sct[i] = transposed(scale_row)
+        own_rows = pl.ds(pl.multiple_of(t * sub, 8), sub)
+        scale = sct[i, own_rows, 0:1]
+        weights = mt[i, own_rows, :]
+        for d in tp_others:
+            remote(part.at[i, d], rsbuf.at[i, d], rs_s.at[i, d], rs_r.at[i, d], at_tp(d)).wait_recv()
+        total = part[i, t].astype(f32)
+        for d in tp_others:
+            total = total + rsbuf[i, d].astype(f32)
+        total = total * scale
+        kinds = top_count + 1
+        for k in range(kinds):
+            gate = total[:, k * units : (k + 1) * units]
+            up = total[:, (kinds + k) * units : (kinds + k + 1) * units]
+            value = jax.nn.silu(gate) * up
+            if k < top_count:
+                value = value * weights[:, top_count + k : top_count + k + 1]
+            hid[i, t, :, k * units : (k + 1) * units] = value.astype(bf16)
+        for d in tp_others:
+            remote(hid.at[i, t], hid.at[i, t], ag_s.at[i, d], ag_r.at[i, t], at_tp(d)).start()
+
+    def down_block(i):
+        for d in tp_others:
+            remote(hid.at[i, d], hid.at[i, d], ag_s.at[i, d], ag_r.at[i, d], at_tp(d)).wait_recv()
+        values = hid[i].astype(f32).reshape(rows, (top_count + 1) * units)
+        names = [mt[i, :, k : k + 1] for k in range(top_count)]
+        spread = []
+        for e in range(experts):
+            chosen = jnp.zeros((rows, units), f32)
+            for k, name in enumerate(names):
+                chosen = jnp.where(name == float(e), values[:, k * units : (k + 1) * units], chosen)
+            spread.append(chosen.astype(bf16))
+        spread.append(values[:, top_count * units :].astype(bf16))
+        weight = wall[2].reshape((experts + 1) * units, width)
+        return jnp.dot(jnp.concatenate(spread, axis=1), weight, preferred_element_type=f32)
+
+    def finish_block(i):
+        product = down_block(i)
+        if i == 0:
+            outf[...] = product
+        else:
+            s = source(i)
+            outb[i] = product.astype(bf16)
+            remote(outb.at[i], retbuf.at[f], ret_s.at[i], ret_r.at[f], at_fs(s)).start()
+
+    def token_block(i):
+        s = source(i)
+        remote(metabuf.at[s], metabuf.at[s], meta_s.at[s, 0], meta_r.at[s], partner).wait_recv()
+        onward(s, metabuf.at[s], meta_s, meta_r)
+        remote(tokbuf.at[s], tokbuf.at[s], tok_s.at[s, 0], tok_r.at[s], partner).wait_recv()
+        onward(s, tokbuf.at[s], tok_s, tok_r)
+
+    def scale_block(i):
+        s = source(i)
+        remote(scown, scbuf.at[s], sc_s.at[s], sc_r.at[s], partner).wait_recv()
+        return scbuf.at[s]
+
+    forward_block(0, tok_ref, meta_ref)
+    squares = ssown[...]
+    for d in tp_others:
+        remote(ssown, ssbuf.at[d], ss_s.at[d], ss_r.at[d], at_tp(d)).wait_recv()
+        squares = squares + ssbuf[d]
+    scown[...] = lax.rsqrt(squares / (width * n_tp) + norm_eps)
+    for d in fs_others:
+        remote(scown, scbuf.at[f], sc_s.at[d], sc_r.at[f], at_fs(d)).start()
+    for e in range(experts):
+        wall[2, e] = ed_ref[e].astype(bf16)
+    wall[2, experts] = sd_ref[...].astype(bf16)
+
+    token_block(1)
+    forward_block(1, tokbuf.at[source(1)], metabuf.at[source(1)])
+    hidden_block(0, scown)
+    for i in range(2, n_fs):
+        token_block(i)
+        if i == n_fs - 1:
+            mine = pl.ds(pl.multiple_of(g * half, 16), half)
+            for way, go in ((0, to_right), (1, to_left)):
+                go(wall.at[:, experts, mine], wout_ref.at[1, :, f, g], ws_s.at[f, way], ws_r.at[f])
+            for d in fs_others:
+                remote(
+                    wall.at[:, d, mine], wout_ref.at[0, :, f, g], we_s.at[d], we_r.at[f], at_fs(d)
+                ).start()
+        forward_block(i, tokbuf.at[source(i)], metabuf.at[source(i)])
+        hidden_block(i - 1, scale_block(i - 1))
+        finish_block(i - 2)
+    for h in range(2):
+        wout_ref[0, :, f, h] = wall[:, f, h * half : (h + 1) * half]
+        wout_ref[1, :, f, h] = wall[:, experts, h * half : (h + 1) * half]
+    hidden_block(n_fs - 1, scale_block(n_fs - 1))
+    finish_block(n_fs - 2)
+    finish_block(n_fs - 1)
+
+    for i in range(1, n_fs):
+        s = source(i)
+        shared, routed = wout_ref.at[1, :, s, g], wout_ref.at[0, :, s, g]
+        remote(shared, shared, ws_s.at[s, 0], ws_r.at[s], partner).wait_recv()
+        onward(s, shared, ws_s, ws_r)
+        remote(shared, shared, ys_s.at[s], ys_r.at[s], partner).start()
+        remote(routed, routed, we_s.at[s], we_r.at[s], partner).wait_recv()
+        remote(routed, routed, ye_s.at[s], ye_r.at[s], partner).start()
+
+    total = outf[...]
+    for d in fs_others:
+        remote(retbuf.at[d], retbuf.at[d], ret_s.at[1], ret_r.at[d], partner).wait_recv()
+        total = total + retbuf[d].astype(f32)
+    mixed_ref[...] = total.astype(bf16)
+
+    for d in fs_others:
+        shared, routed = wout_ref.at[1, :, d, 1 - g], wout_ref.at[0, :, d, 1 - g]
+        remote(shared, shared, ys_s.at[d], ys_r.at[d], partner).wait_recv()
+        remote(routed, routed, ye_s.at[d], ye_r.at[d], partner).wait_recv()
+
+    line_sends_done(lambda s: metabuf.at[s], meta_s, meta_r)
+    line_sends_done(lambda s: tokbuf.at[s], tok_s, tok_r)
+    line_sends_done(lambda s: wout_ref.at[1, :, s, g], ws_s, ws_r)
+    for d in tp_others:
+        remote(ssown, ssbuf.at[t], ss_s.at[d], ss_r.at[t], at_tp(d)).wait_send()
+        for i in range(n_fs):
+            remote(part.at[i, d], rsbuf.at[i, t], rs_s.at[i, d], rs_r.at[i, t], at_tp(d)).wait_send()
+            remote(hid.at[i, t], hid.at[i, t], ag_s.at[i, d], ag_r.at[i, t], at_tp(d)).wait_send()
+    for j, d in enumerate(fs_others):
+        remote(scown, scbuf.at[f], sc_s.at[d], sc_r.at[f], at_fs(d)).wait_send()
+        remote(outb.at[j + 1], retbuf.at[f], ret_s.at[j + 1], ret_r.at[f], at_fs(d)).wait_send()
+        shared, routed = wout_ref.at[1, :, d, g], wout_ref.at[0, :, d, g]
+        remote(routed, routed, we_s.at[d], we_r.at[f], at_fs(d)).wait_send()
+        remote(shared, shared, ys_s.at[d], ys_r.at[d], partner).wait_send()
+        remote(routed, routed, ye_s.at[d], ye_r.at[d], partner).wait_send()
+
+
+def per_device_fused(
+    tokens,
+    routes,
+    routing_weight,
+    norm_gain_vector,
+    expert_gate,
+    expert_up,
+    expert_down,
+    shared_gate,
+    shared_up,
+    shared_down,
+):
+    n_fs, n_tp = lax.axis_size("fs"), lax.axis_size("tp")
+    rows, width = tokens.shape
+    experts, units, _ = expert_gate.shape
+    top_count = routes.shape[1]
+    sub, half = rows // n_tp, units // 2
+    meta_rows = -(-2 * top_count // 8) * 8
+    lanes = -(-rows // 128) * 128
+    meta = jnp.concatenate([routes.astype(jnp.float32), routing_weight], axis=1).T
+    meta = jnp.pad(meta, ((0, meta_rows - 2 * top_count), (0, lanes - rows)))
+    f32, bf16 = jnp.float32, jnp.bfloat16
+    kinds = top_count + 1
+    dma = pltpu.SemaphoreType.DMA
+    vmem = pl.BlockSpec(memory_space=pltpu.VMEM)
+    mixed, served = pl.pallas_call(
+        functools.partial(fused_kernel, n_fs, n_tp, top_count),
+        out_shape=(
+            jax.ShapeDtypeStruct((rows, width), bf16),
+            jax.ShapeDtypeStruct((2, 3, n_fs, 2, half, width), bf16),
+        ),
+        in_specs=[vmem] * 9,
+        out_specs=(vmem, vmem),
+        scratch_shapes=[
+            pltpu.VMEM((3, experts + 1, units, width), bf16),
+            pltpu.VMEM((n_fs, rows, width), bf16),
+            pltpu.VMEM((n_fs, meta_rows, lanes), f32),
+            pltpu.VMEM((8, lanes), f32),
+            pltpu.VMEM((n_tp, 8, lanes), f32),
+            pltpu.VMEM((8, lanes), f32),
+            pltpu.VMEM((n_fs, 8, lanes), f32),
+            pltpu.VMEM((n_fs, rows, meta_rows), f32),
+            pltpu.VMEM((n_fs, rows, 8), f32),
+            pltpu.VMEM((n_fs, n_tp, sub, 2 * kinds * units), bf16),
+            pltpu.VMEM((n_fs, n_tp, sub, 2 * kinds * units), bf16),
+            pltpu.VMEM((n_fs, n_tp, sub, kinds * units), bf16),
+            pltpu.VMEM((rows, width), f32),
+            pltpu.VMEM((n_fs, rows, width), bf16),
+            pltpu.VMEM((n_fs, rows, width), bf16),
+            dma((n_fs, 2)), dma((n_fs,)),
+            dma((n_fs, 2)), dma((n_fs,)),
+            dma((n_tp,)), dma((n_tp,)),
+            dma((n_fs,)), dma((n_fs,)),
+            dma((n_fs, n_tp)), dma((n_fs, n_tp)),
+            dma((n_fs, n_tp)), dma((n_fs, n_tp)),
+            dma((n_fs,)), dma((n_fs,)),
+            dma((n_fs,)), dma((n_fs,)),
+            dma((n_fs, 2)), dma((n_fs,)),
+            dma((n_fs,)), dma((n_fs,)),
+            dma((n_fs,)), dma((n_fs,)),
+        ],
+        compiler_params=pltpu.CompilerParams(
+            collective_id=0, has_side_effects=True, vmem_limit_bytes=60 * 1024 * 1024
+        ),
+        name="hand_over_and_layer",
+    )(
+        tokens, meta, norm_gain_vector[None, :],
+        expert_gate, expert_up, expert_down, shared_gate, shared_up, shared_down,
+    )
+    served = served.reshape(2, 3, n_fs * units, width)
+    return (
+        mixed,
+        served[0, 0][None], served[0, 1][None], served[0, 2][None],
+        served[1, 0], served[1, 1], served[1, 2],
+    )
+
+
+def per_device(tokens, routes, routing_weight, norm_gain_vector, *weights):
+    experts, units, width = weights[0].shape
+    rows, n_fs, n_tp = tokens.shape[0], lax.axis_size("fs"), lax.axis_size("tp")
+    whole_tiles = units % 128 == 0 and width % 128 == 0 and rows % (16 * n_tp) == 0
+    fits = (experts + 1) * units * width <= 2**20 and n_fs <= 4 and n_tp <= 4
+    chosen = per_device_plain
+    if whole_tiles and fits and experts == n_fs and lax.axis_size("grp") == 2 and n_fs > 2:
+        chosen = per_device_fused
+    return chosen(tokens, routes, routing_weight, norm_gain_vector, *weights)
+
+
 def solution(mesh):
     return jax.shard_map(
         per_device,

time: 187 us -> 92 us (0.49)
  blocking collectives: 99.9 us -> 0 us
  Pallas kernels: 0 us -> 85 us
  waiting for transfers between devices: 21.6 us -> 0 us
  starting transfers between devices: 17.6 us -> 0 us
  local copies, waits for them, and re-layouts: 20.8 us -> 4.85 us
  between operations: 14 us -> 0.65 us
  other arithmetic: 7.37 us -> 1.37 us
  matrix products: 4.78 us -> 0 us
    pallas_call x0 -> x1, Pallas kernels: none -> 85 us  [per_device_fused(): pl.pallas_call(functools.partial(fused_kernel, n_fs, n_tp, top_count), ou...]
    all_gather x5 -> x0, blocking collectives: 75.6 us -> none  [the longest x1 24.3 us: per_device(): lax.all_gather((shared_gate * norm_gain_vector[None, :]).astype(jnp.bfloa...]
    all_to_all x4 -> x0, waiting for transfers between devices: 21.4 us -> none  [the longest x1 11.8 us: per_device(): lax.all_to_all(up_round, 'fs', split_axis=0, concat_axis=1, tiled=True)]
    all_to_all x4 -> x0, starting transfers between devices: 17.4 us -> none  [the longest x1 5.37 us: per_device(): lax.all_to_all(produced.reshape(experts, capacity, portion_width), 'fs',...]
    all_to_all x1 -> x0, blocking collectives: 15.7 us -> none  [per_device(): lax.all_to_all(gate_round, 'fs', split_axis=0, concat_axis=1, tiled=True)]
    unnamed x38 -> x3, local copies, waits for them, and re-layouts: 15.7 us -> 0.68 us
    psum x1 -> x0, blocking collectives: 8.5 us -> none  [per_device(): totals = lax.psum(jnp.sum(values * values, axis=1), 'tp')]
    dot_general x7 -> x0, matrix products: 4.78 us -> none  [the longest x4 1.52 us: dense_rows(): lax.dot_general(rows, weight, (((1,), (1,)), ((), ())), preferred_element...]
  transfers between devices with their start and end apart: 8 -> 0, of which waited for: 2 -> 0; matrix products, arithmetic and copies ran while one was open for 8% -> 0% of each run, Pallas kernels for 0% -> 0%
where the time goes in v1:
time: 92 us; the launch traced here: 91.8 us
  Pallas kernels  85 us (92%)
  local copies, waits for them, and re-layouts  4.85 us (5%)
  other arithmetic  1.37 us (1%)
    pallas_call x1, Pallas kernels, per_device_fused(): pl.pallas_call(functools.partial(fused_kernel, n_fs, n_tp, top_count), ou...  85 us
    squeeze x1, local copies, waits for them, and re-layouts, per_device_fused(): served[1, 2]  3.56 us

profile of v1, /device:TPU:0, one launch (start us, length us, event | category | flops | bytes accessed | tf_op | source)
XLA Modules:
  0.0 91.8 jit_solution(18901969460466946)
XLA Ops:
  0.6 0.7 convert_element_type.5
  1.3 0.7 maximum_bitcast_fusion
  2.0 0.6 pad.4.meta_ref
  2.6 85.0 %hand_over_and_layer.1 = (bf16[192,512]{1,0:T(8,128)(2,1)}, bf16[2,3,4,2,64,512]{5,4,3,2,1,0:T(8,128)(2,1)}) custom-call(bf16[192,512]{1,0:T(8,128)(2,1)} %tok_ref.1, f32[8,256]{1,0:T(8,128)} %pad.4.meta_ref, f32[1,512]{1,0:T(1,128)} %bitcast.17, f32[4,128,512]{2,1,0:T(8,128)} %eg_ref.1, f32[4,128,512]{2,1,0:T(8,128)} %eu_ref.1, f32[4,128,512]{2,1,0:T(8,128)} %ed_ref.1, ...), custom_call_target="tpu_custom_call" | custom-call | tf_op jit(solution)/shard_map/hand_over_and_layer/pallas_call | solution.py:397
  87.6 0.0 copy-start
  87.6 3.6 %slice_bitcast_fusion = (bf16[512,512]{1,0:T(8,128)(2,1)}, bf16[512,512]{1,0:T(8,128)(2,1)}, bf16[512,512]{1,0:T(8,128)(2,1)}, bf16[1,512,512]{2,1,0:T(8,128)(2,...) fusion(bf16[2,3,512,512]{3,2,1,0:T(8,128)(2,1)} %bitcast.16), kind=kLoop, calls=%fused_computation | loop fusion | bytes 6291456 | tf_op jit(solution)/shard_map/squeeze | solution.py:445
  91.2 0.0 copy-done
  91.2 0.7 copy.18
Async XLA Ops:
  87.6 3.6 %copy-start = (bf16[192,512]{1,0:T(8,128)(2,1)S(1)}, bf16[192,512]{1,0:T(8,128)(2,1)}, u32[]{:S(2)}) copy-start(bf16[192,512]{1,0:T(8,128)(2,1)} %get-tuple-element.24) | copy-start | bytes 589828

commit v2 on v1

--- a/solution.py
+++ b/solution.py
@@ -120,9 +120,9 @@
 
 def fused_kernel(
     n_fs, n_tp, top_count,
-    tok_ref, meta_ref, gain_ref, eg_ref, eu_ref, ed_ref, sg_ref, su_ref, sd_ref,
+    tok_ref, routes_ref, weight_ref, gain_ref, eg_ref, eu_ref, ed_ref, sg_ref, su_ref, sd_ref,
     mixed_ref, wout_ref,
-    wall, tokbuf, metabuf, ssown, ssbuf, scown, scbuf, mt, sct, part, rsbuf, hid, outf, outb, retbuf,
+    wall, tokbuf, meta_ref, metabuf, ssown, ssbuf, scown, scbuf, mt, sct, part, rsbuf, hid, outf, outb, retbuf,
     tok_s, tok_r, meta_s, meta_r, ss_s, ss_r, sc_s, sc_r, rs_s, rs_r, ag_s, ag_r,
     ret_s, ret_r, we_s, we_r, ws_s, ws_r, ye_s, ye_r, ys_s, ys_r,
 ):
@@ -197,6 +197,9 @@
             def _():
                 remote(ref, ref, send.at[s, 1], recv.at[s], at_fs(f - 1)).wait_send()
 
+    meta_ref[...] = jnp.zeros(meta_ref.shape, f32)
+    meta_ref[0:top_count, 0:rows] = routes_ref[...].astype(f32)
+    meta_ref[top_count : 2 * top_count, 0:rows] = weight_ref[...]
     for go, way in ((to_right, 0), (to_left, 1)):
         go(meta_ref, metabuf.at[f], meta_s.at[f, way], meta_r.at[f])
         go(tok_ref, tokbuf.at[f], tok_s.at[f, way], tok_r.at[f])
@@ -297,6 +300,33 @@
         remote(scown, scbuf.at[s], sc_s.at[s], sc_r.at[s], partner).wait_recv()
         return scbuf.at[s]
 
+    for e in range(experts):
+        wall[2, e] = ed_ref[e].astype(bf16)
+    wall[2, experts] = sd_ref[...].astype(bf16)
+
+    mine = pl.ds(pl.multiple_of(g * half, 16), half)
+    for way, go in ((0, to_right), (1, to_left)):
+        go(wall.at[:, experts, mine], wout_ref.at[1, :, f, g], ws_s.at[f, way], ws_r.at[f])
+
+    def give_expert(i):
+        d = source(i)
+        remote(
+            wall.at[:, d, mine], wout_ref.at[0, :, f, g], we_s.at[d], we_r.at[f], at_fs(d)
+        ).start()
+
+    def pass_shared(i):
+        s = source(i)
+        shared = wout_ref.at[1, :, s, g]
+        remote(shared, shared, ws_s.at[s, 0], ws_r.at[s], partner).wait_recv()
+        onward(s, shared, ws_s, ws_r)
+        remote(shared, shared, ys_s.at[s], ys_r.at[s], partner).start()
+
+    def pass_routed(i):
+        s = source(i)
+        routed = wout_ref.at[0, :, s, g]
+        remote(routed, routed, we_s.at[s], we_r.at[s], partner).wait_recv()
+        remote(routed, routed, ye_s.at[s], ye_r.at[s], partner).start()
+
     forward_block(0, tok_ref, meta_ref)
     squares = ssown[...]
     for d in tp_others:
@@ -305,41 +335,25 @@
     scown[...] = lax.rsqrt(squares / (width * n_tp) + norm_eps)
     for d in fs_others:
         remote(scown, scbuf.at[f], sc_s.at[d], sc_r.at[f], at_fs(d)).start()
-    for e in range(experts):
-        wall[2, e] = ed_ref[e].astype(bf16)
-    wall[2, experts] = sd_ref[...].astype(bf16)
-
-    token_block(1)
-    forward_block(1, tokbuf.at[source(1)], metabuf.at[source(1)])
-    hidden_block(0, scown)
-    for i in range(2, n_fs):
-        token_block(i)
-        if i == n_fs - 1:
-            mine = pl.ds(pl.multiple_of(g * half, 16), half)
-            for way, go in ((0, to_right), (1, to_left)):
-                go(wall.at[:, experts, mine], wout_ref.at[1, :, f, g], ws_s.at[f, way], ws_r.at[f])
-            for d in fs_others:
-                remote(
-                    wall.at[:, d, mine], wout_ref.at[0, :, f, g], we_s.at[d], we_r.at[f], at_fs(d)
-                ).start()
-        forward_block(i, tokbuf.at[source(i)], metabuf.at[source(i)])
-        hidden_block(i - 1, scale_block(i - 1))
-        finish_block(i - 2)
     for h in range(2):
         wout_ref[0, :, f, h] = wall[:, f, h * half : (h + 1) * half]
         wout_ref[1, :, f, h] = wall[:, experts, h * half : (h + 1) * half]
+
+    for i in range(1, n_fs):
+        token_block(i)
+        give_expert(i)
+        forward_block(i, tokbuf.at[source(i)], metabuf.at[source(i)])
+        hidden_block(i - 1, scown if i == 1 else scale_block(i - 1))
+        if i >= 2:
+            finish_block(i - 2)
+            pass_shared(i - 1)
+    pass_routed(1)
     hidden_block(n_fs - 1, scale_block(n_fs - 1))
     finish_block(n_fs - 2)
     finish_block(n_fs - 1)
-
-    for i in range(1, n_fs):
-        s = source(i)
-        shared, routed = wout_ref.at[1, :, s, g], wout_ref.at[0, :, s, g]
-        remote(shared, shared, ws_s.at[s, 0], ws_r.at[s], partner).wait_recv()
-        onward(s, shared, ws_s, ws_r)
-        remote(shared, shared, ys_s.at[s], ys_r.at[s], partner).start()
-        remote(routed, routed, we_s.at[s], we_r.at[s], partner).wait_recv()
-        remote(routed, routed, ye_s.at[s], ye_r.at[s], partner).start()
+    pass_shared(n_fs - 1)
+    for i in range(2, n_fs):
+        pass_routed(i)
 
     total = outf[...]
     for d in fs_others:
@@ -388,8 +402,6 @@
     sub, half = rows // n_tp, units // 2
     meta_rows = -(-2 * top_count // 8) * 8
     lanes = -(-rows // 128) * 128
-    meta = jnp.concatenate([routes.astype(jnp.float32), routing_weight], axis=1).T
-    meta = jnp.pad(meta, ((0, meta_rows - 2 * top_count), (0, lanes - rows)))
     f32, bf16 = jnp.float32, jnp.bfloat16
     kinds = top_count + 1
     dma = pltpu.SemaphoreType.DMA
@@ -400,11 +412,12 @@
             jax.ShapeDtypeStruct((rows, width), bf16),
             jax.ShapeDtypeStruct((2, 3, n_fs, 2, half, width), bf16),
         ),
-        in_specs=[vmem] * 9,
+        in_specs=[vmem] * 10,
         out_specs=(vmem, vmem),
         scratch_shapes=[
             pltpu.VMEM((3, experts + 1, units, width), bf16),
             pltpu.VMEM((n_fs, rows, width), bf16),
+            pltpu.VMEM((meta_rows, lanes), f32),
             pltpu.VMEM((n_fs, meta_rows, lanes), f32),
             pltpu.VMEM((8, lanes), f32),
             pltpu.VMEM((n_tp, 8, lanes), f32),
@@ -435,7 +448,7 @@
         ),
         name="hand_over_and_layer",
     )(
-        tokens, meta, norm_gain_vector[None, :],
+        tokens, routes.T, routing_weight.T, norm_gain_vector[None, :],
         expert_gate, expert_up, expert_down, shared_gate, shared_up, shared_down,
     )
     served = served.reshape(2, 3, n_fs * units, width)

time: 92 us -> 87.9 us (0.955)
  Pallas kernels: 85 us -> 82.8 us
  other arithmetic: 1.37 us -> 0 us
    pallas_call x1, Pallas kernels: 85 us -> 82.8 us  [per_device_fused(): pl.pallas_call(functools.partial(fused_kernel, n_fs, n_tp, top_count), ou...]
where the time goes in v2:
time: 87.9 us; the launch traced here: 87.7 us
  Pallas kernels  82.8 us (94%)
  local copies, waits for them, and re-layouts  4.24 us (5%)
    pallas_call x1, Pallas kernels, per_device_fused(): pl.pallas_call(functools.partial(fused_kernel, n_fs, n_tp, top_count), ou...  82.8 us
    squeeze x1, local copies, waits for them, and re-layouts, per_device_fused(): served[1, 2]  3.56 us

profile of v2, /device:TPU:0, one launch (start us, length us, event | category | flops | bytes accessed | tf_op | source)
XLA Modules:
  0.0 87.7 jit_solution(13979393654172746758)
XLA Ops:
  0.6 82.8 %hand_over_and_layer.1 = (bf16[192,512]{1,0:T(8,128)(2,1)}, bf16[2,3,4,2,64,512]{5,4,3,2,1,0:T(8,128)(2,1)}) custom-call(bf16[192,512]{1,0:T(8,128)(2,1)} %tok_ref.1, s32[2,192]{1,0:T(2,128)} %bitcast.17, f32[2,192]{1,0:T(2,128)} %bitcast.18, f32[1,512]{1,0:T(1,128)} %bitcast.19, f32[4,128,512]{2,1,0:T(8,128)} %eg_ref.1, f32[4,128,512]{2,1,0:T(8,128)} %eu_ref.1, ...), custom_call_target="tpu_custom_call" | custom-call | tf_op jit(solution)/shard_map/hand_over_and_layer/pallas_call | solution.py:409
  83.5 0.0 copy-start
  83.5 3.6 %slice_bitcast_fusion = (bf16[512,512]{1,0:T(8,128)(2,1)}, bf16[512,512]{1,0:T(8,128)(2,1)}, bf16[512,512]{1,0:T(8,128)(2,1)}, bf16[1,512,512]{2,1,0:T(8,128)(2,...) fusion(bf16[2,3,512,512]{3,2,1,0:T(8,128)(2,1)} %bitcast.16), kind=kLoop, calls=%fused_computation | loop fusion | bytes 6291456 | tf_op jit(solution)/shard_map/squeeze | solution.py:458
  87.0 0.0 copy-done
  87.0 0.7 copy.18
Async XLA Ops:
  83.5 3.6 %copy-start = (bf16[192,512]{1,0:T(8,128)(2,1)S(1)}, bf16[192,512]{1,0:T(8,128)(2,1)}, u32[]{:S(2)}) copy-start(bf16[192,512]{1,0:T(8,128)(2,1)} %get-tuple-element.24) | copy-start | bytes 589828

commit v3 on v2

--- a/solution.py
+++ b/solution.py
@@ -341,18 +341,18 @@
 
     for i in range(1, n_fs):
         token_block(i)
-        give_expert(i)
+        give_expert(n_fs - i)
         forward_block(i, tokbuf.at[source(i)], metabuf.at[source(i)])
         hidden_block(i - 1, scown if i == 1 else scale_block(i - 1))
         if i >= 2:
             finish_block(i - 2)
             pass_shared(i - 1)
-    pass_routed(1)
+    pass_routed(n_fs - 1)
     hidden_block(n_fs - 1, scale_block(n_fs - 1))
     finish_block(n_fs - 2)
     finish_block(n_fs - 1)
     pass_shared(n_fs - 1)
-    for i in range(2, n_fs):
+    for i in range(n_fs - 2, 0, -1):
         pass_routed(i)
 
     total = outf[...]

time: 87.9 us -> 91.1 us (1.036)
  Pallas kernels: 82.8 us -> 86.1 us
    pallas_call x1, Pallas kernels: 82.8 us -> 86.1 us  [per_device_fused(): pl.pallas_call(functools.partial(fused_kernel, n_fs, n_tp, top_count), ou...]
where the time goes in v3:
time: 91.1 us; the launch traced here: 91 us
  Pallas kernels  86.1 us (95%)
  local copies, waits for them, and re-layouts  4.24 us (5%)
    pallas_call x1, Pallas kernels, per_device_fused(): pl.pallas_call(functools.partial(fused_kernel, n_fs, n_tp, top_count), ou...  86.1 us
    squeeze x1, local copies, waits for them, and re-layouts, per_device_fused(): served[1, 2]  3.56 us

profile of v3, /device:TPU:0, one launch (start us, length us, event | category | flops | bytes accessed | tf_op | source)
XLA Modules:
  0.0 91.0 jit_solution(15060291643809868438)
XLA Ops:
  0.6 86.1 %hand_over_and_layer.1 = (bf16[192,512]{1,0:T(8,128)(2,1)}, bf16[2,3,4,2,64,512]{5,4,3,2,1,0:T(8,128)(2,1)}) custom-call(bf16[192,512]{1,0:T(8,128)(2,1)} %tok_ref.1, s32[2,192]{1,0:T(2,128)} %bitcast.17, f32[2,192]{1,0:T(2,128)} %bitcast.18, f32[1,512]{1,0:T(1,128)} %bitcast.19, f32[4,128,512]{2,1,0:T(8,128)} %eg_ref.1, f32[4,128,512]{2,1,0:T(8,128)} %eu_ref.1, ...), custom_call_target="tpu_custom_call" | custom-call | tf_op jit(solution)/shard_map/hand_over_and_layer/pallas_call | solution.py:409
  86.8 0.0 copy-start
  86.8 3.6 %slice_bitcast_fusion = (bf16[512,512]{1,0:T(8,128)(2,1)}, bf16[512,512]{1,0:T(8,128)(2,1)}, bf16[512,512]{1,0:T(8,128)(2,1)}, bf16[1,512,512]{2,1,0:T(8,128)(2,...) fusion(bf16[2,3,512,512]{3,2,1,0:T(8,128)(2,1)} %bitcast.16), kind=kLoop, calls=%fused_computation | loop fusion | bytes 6291456 | tf_op jit(solution)/shard_map/squeeze | solution.py:458
  90.3 0.0 copy-done
  90.3 0.7 copy.18
Async XLA Ops:
  86.8 3.6 %copy-start = (bf16[192,512]{1,0:T(8,128)(2,1)S(1)}, bf16[192,512]{1,0:T(8,128)(2,1)}, u32[]{:S(2)}) copy-start(bf16[192,512]{1,0:T(8,128)(2,1)} %get-tuple-element.24) | copy-start | bytes 589828
